TPU v7x, 32 devices: a whole 2x2x4 slice. The times are simulated.
32 devices in a mesh: grp: 2 (over y), ra: 4 (over z), cb: 4 (over x, core).
Axes of the slice: x: 2, y: 2, z: 4, core: 2. Of those that a mesh axis runs over, the one named last changes fastest.
Arguments:
- tokens: bfloat16 [256, 2048], P('grp', 'ra'), parts along dimension 0, may hold values from -8 to 8
- first_gain: bfloat16 [2048], P('ra'), may hold values from 0.099609375 to 1.8984375
- first_gate: bfloat16 [2048, 5632], P('ra', 'cb'), may hold values from -0.125 to 0.125
- first_up: bfloat16 [2048, 5632], P('ra', 'cb'), may hold values from -0.125 to 0.125
- first_down: bfloat16 [5632, 2048], P('cb', 'ra'), may hold values from -0.078125 to 0.078125
- second_gain: bfloat16 [2048], P('ra'), may hold values from 0.099609375 to 1.8984375
- second_gate: bfloat16 [2048, 5632], P('ra', 'cb'), may hold values from -0.125 to 0.125
- second_up: bfloat16 [2048, 5632], P('ra', 'cb'), may hold values from -0.125 to 0.125
- second_down: bfloat16 [5632, 2048], P('cb', 'ra'), may hold values from -0.078125 to 0.078125
Outputs:
- latent_out: bfloat16 [256, 2048], P('grp', 'ra'), parts along dimension 0
There are 2 independent parts, one for each index of `grp`. A program takes and returns all parts, laid end to end along the dimension named above; an argument that names none is the same for every part. Nothing has to cross between parts.
All inputs are finite; a program needn't handle non-finite values.
Results may differ from a plain program's by a relative error of at most 0.0088.
Values may be sent and summed in bfloat16 or wider, within the bound.
No kernel may reach another device: no remote copies, remote signals or barrier semaphores. Data moves between devices by JAX's collectives and lax.ppermute only.
A program may use at most 64 MiB of HBM per device.

v0:
```python
import jax
import jax.numpy as jnp
from jax import lax
from jax.sharding import PartitionSpec as P


def sublayer(x, gain, w_gate, w_up, w_down):
    xf = x.astype(jnp.float32)
    width = x.shape[1] * lax.axis_size("ra")
    rows = x.shape[0]
    squares = jnp.sum(xf * xf, axis=1)
    normed = (xf * gain.astype(jnp.float32)).astype(jnp.bfloat16)
    dims = (((0,), (1,)), ((), ()))
    gate_rows = lax.dot_general(w_gate, normed, dims, preferred_element_type=jnp.float32)
    up_rows = lax.dot_general(w_up, normed, dims, preferred_element_type=jnp.float32)
    shares = lax.psum_scatter(
        jnp.concatenate([gate_rows, up_rows], axis=1), "ra", scatter_dimension=0, tiled=True
    )
    total_sq = lax.psum(squares, "ra")
    scale = lax.rsqrt(total_sq / width + 1e-06)
    hidden_t = (
        jax.nn.silu(shares[:, :rows] * scale[None, :]) * (shares[:, rows:] * scale[None, :])
    ).astype(jnp.bfloat16)
    partial_value = lax.dot_general(
        lax.all_gather(hidden_t, "ra", axis=0, tiled=True),
        w_down,
        (((0,), (0,)), ((), ())),
        preferred_element_type=jnp.float32,
    )
    branch = lax.psum(partial_value, "cb")
    return (0.5 * xf + 0.5 * branch).astype(jnp.bfloat16)


def per_device(
    tokens,
    first_gain,
    first_gate,
    first_up,
    first_down,
    second_gain,
    second_gate,
    second_up,
    second_down,
):
    middle = sublayer(tokens, first_gain, first_gate, first_up, first_down)
    return sublayer(middle, second_gain, second_gate, second_up, second_down)


def solution(mesh):
    placed = (
        P("grp", "ra"),
        P("ra"),
        P("ra", "cb"),
        P("ra", "cb"),
        P("cb", "ra"),
        P("ra"),
        P("ra", "cb"),
        P("ra", "cb"),
        P("cb", "ra"),
    )
    return jax.shard_map(
        per_device, mesh=mesh, in_specs=placed, out_specs=P("grp", "ra"), check_vma=False
    )
```

profile of v0, /device:TPU:0, one launch (start us, length us, event | category | flops | bytes accessed | tf_op | source)
XLA Modules:
  0.0 194.4 jit_solution(9216063514448310554)
XLA Ops:
  6.5 0.0 copy-start
  6.5 0.0 copy-start.1
  6.5 0.0 copy-start.2
  6.5 0.0 reduce-scatter.7.cloned.1.call-start
  6.5 0.8 convert_element_type.31
  7.4 0.5 copy-done
  7.9 1.3 convolution_bitcast_fusion.2
  9.2 0.0 copy-done.1
  9.2 0.0 copy-done.2
  9.2 0.4 convolution_bitcast_fusion.3
  9.6 0.1 pad_maximum_fusion
  9.7 1.6 copy.12
  11.3 0.0 reduce-scatter.7.cloned.1.call-update
  11.3 0.0 copy-start.3
  11.3 0.0 all-reduce.3.cloned.1.call-start
  11.3 0.1 fusion.1
  11.5 13.6 %psum.28 = f32[128]{0:T(128)S(1)} all-reduce(f32[128]{0:T(128)S(1)} %fusion.1), channel_id=1, replica_groups=mesh['grp'=2,'ra'=4,'cb'=4] {'ra'}, use_global_device_ids=true, to_apply=%region_2.0 | all-reduce | flops 128 | bytes 1024 | tf_op jit(solution)/shard_map/psum | solution.py:19
  25.1 22.5 %reduce-scatter.7.cloned.1.call-done = f32[352,256]{1,0:T(8,128)} async-done(((f32[1408,256]{1,0:T(8,128)}), f32[352,256]{1,0:T(8,128)}) %reduce-scatter.7.cloned.1.call-update) | async-done | bytes 360464
  47.6 1.7 fusion.14
  49.3 0.1 copy.16
  49.4 1.1 copy.17
  50.5 0.1 multiply_convert_fusion.1
  50.6 0.0 copy-start.6
  50.6 0.1 copy.10
  50.8 15.0 %all_gather.6 = bf16[1408,128]{1,0:T(8,128)(2,1)S(1)} all-gather(bf16[352,128]{1,0:T(8,128)(2,1)S(1)} %copy.10), channel_id=1, replica_groups=mesh['grp'=2,'ra'=4,'cb'=4] {'ra'}, dimensions={0}, use_global_device_ids=true | all-gather | bytes 450560 | tf_op jit(solution)/shard_map/all_gather | solution.py:25
  65.8 0.0 copy-done.3
  65.8 1.1 fusion.15
  66.9 0.0 all-reduce.3.cloned.1.call-update
  66.9 0.0 copy-start.4
  66.9 0.0 reduce-scatter.9.cloned.1.call-start
  67.0 0.0 copy-done.6
  67.0 30.7 %all-reduce.3.cloned.1.call-done = f32[128,512]{1,0:T(8,128)} async-done(((f32[128,512]{1,0:T(8,128)}), f32[128,512]{1,0:T(8,128)}) %all-reduce.3.cloned.1.call-update) | async-done | bytes 262160 | tf_op jit(solution)/shard_map/psum | solution.py:30
  97.7 1.1 fusion.5
  98.8 1.7 convolution_bitcast_fusion
  100.5 0.0 copy-done.4
  100.5 0.4 convolution_bitcast_fusion.1
  100.9 0.1 pad_maximum_fusion.1
  101.0 1.6 copy.14
  102.6 0.0 reduce-scatter.9.cloned.1.call-update
  102.6 0.0 copy-start.5
  102.6 0.0 all-reduce.5.cloned.1.call-start
  102.6 12.1 %psum.30 = f32[128]{0:T(128)S(1)} all-reduce(f32[128]{0:T(128)S(1)} %get-tuple-element.5), channel_id=1, replica_groups=mesh['grp'=2,'ra'=4,'cb'=4] {'ra'}, use_global_device_ids=true, to_apply=%region_6.7 | all-reduce | flops 128 | bytes 1024 | tf_op jit(solution)/shard_map/psum | solution.py:19
  114.7 21.5 %reduce-scatter.9.cloned.1.call-done = f32[352,256]{1,0:T(8,128)} async-done(((f32[1408,256]{1,0:T(8,128)}), f32[352,256]{1,0:T(8,128)}) %reduce-scatter.9.cloned.1.call-update) | async-done | bytes 360464
  136.2 1.7 fusion.13
  137.9 0.1 copy.18
  138.0 1.1 copy.19
  139.1 0.1 multiply_convert_fusion
  139.2 0.1 copy.11
  139.3 15.1 %all_gather.7 = bf16[1408,128]{1,0:T(8,128)(2,1)S(1)} all-gather(bf16[352,128]{1,0:T(8,128)(2,1)S(1)} %copy.11), channel_id=1, replica_groups=mesh['grp'=2,'ra'=4,'cb'=4] {'ra'}, dimensions={0}, use_global_device_ids=true | all-gather | bytes 450560 | tf_op jit(solution)/shard_map/all_gather | solution.py:25
  154.4 0.0 copy-done.5
  154.4 1.1 fusion.16
  155.5 0.0 all-reduce.5.cloned.1.call-update
  155.5 30.7 %all-reduce.5.cloned.1.call-done = f32[128,512]{1,0:T(8,128)} async-done(((f32[128,512]{1,0:T(8,128)}), f32[128,512]{1,0:T(8,128)}) %all-reduce.5.cloned.1.call-update) | async-done | bytes 262160 | tf_op jit(solution)/shard_map/psum | solution.py:30
  186.2 1.6 fusion.7
  (3 shorter events, 0.0 us)
Async XLA Ops:
  6.5 1.4 copy-start
  6.5 2.7 %copy-start.1 = (bf16[128,512]{1,0:T(8,128)(2,1)S(1)}, bf16[128,512]{1,0:T(8,128)(2,1)}, u32[]{:S(2)}) copy-start(bf16[128,512]{1,0:T(8,128)(2,1)} %param.9) | copy-start | bytes 393220
  6.5 2.7 %copy-start.2 = (bf16[512,1408]{1,0:T(8,128)(2,1)S(1)}, bf16[512,1408]{1,0:T(8,128)(2,1)}, u32[]{:S(2)}) copy-start(bf16[512,1408]{1,0:T(8,128)(2,1)} %param.11) | copy-start | bytes 4325380
  6.5 41.1 %reduce-scatter.7.cloned.1.call-start = ((), (), s32[]{:S(2)}) async-start(), calls=%async_computation.4 | async-start | bytes 1802240
  11.3 54.5 %copy-start.3 = (bf16[1408,512]{1,0:T(8,128)(2,1)S(1)}, bf16[1408,512]{1,0:T(8,128)(2,1)}, u32[]{:S(2)}) copy-start(bf16[1408,512]{1,0:T(8,128)(2,1)} %param.13) | copy-start | bytes 4325380
  11.3 86.4 %all-reduce.3.cloned.1.call-start = ((), (), s32[]{:S(2)}) async-start(), calls=%async_computation.2 | async-start | bytes 524288 | tf_op jit(solution)/shard_map/psum | solution.py:30
  50.6 16.3 %copy-start.6 = (bf16[512]{0:T(512)(128)(2,1)S(1)}, bf16[512]{0:T(512)(128)(2,1)}, u32[]{:S(2)}) copy-start(bf16[512]{0:T(512)(128)(2,1)} %param.14) | copy-start | bytes 3076
  66.9 33.6 %copy-start.4 = (bf16[512,1408]{1,0:T(8,128)(2,1)S(1)}, bf16[512,1408]{1,0:T(8,128)(2,1)}, u32[]{:S(2)}) copy-start(bf16[512,1408]{1,0:T(8,128)(2,1)} %param.15) | copy-start | bytes 4325380
  66.9 69.3 %reduce-scatter.9.cloned.1.call-start = ((), (), s32[]{:S(2)}) async-start(), calls=%async_computation.5 | async-start | bytes 1802240
  102.6 51.8 %copy-start.5 = (bf16[1408,512]{1,0:T(8,128)(2,1)S(1)}, bf16[1408,512]{1,0:T(8,128)(2,1)}, u32[]{:S(2)}) copy-start(bf16[1408,512]{1,0:T(8,128)(2,1)} %param.17) | copy-start | bytes 4325380
  102.6 83.6 %all-reduce.5.cloned.1.call-start = ((), (), s32[]{:S(2)}) async-start(), calls=%async_computation.3 | async-start | bytes 524288 | tf_op jit(solution)/shard_map/psum | solution.py:30
Sparse Core Ops, SparseCore 0:
  11.4 36.1 reduce-scatter.6
  67.0 30.5 all-reduce.2
  102.7 33.4 reduce-scatter.8
  155.7 30.5 all-reduce.4
where the time goes:
time: 195 us; the launch traced here: 194 us
  waiting for transfers between devices  105 us (54%)
  blocking collectives  55.8 us (29%)
  between operations  13.3 us (7%)
  local copies, waits for them, and re-layouts  9.67 us (5%)
  matrix products  6.01 us (3%)
  other arithmetic  4.14 us (2%)
    psum x2, waiting for transfers between devices, sublayer(): branch = lax.psum(partial_value, 'cb')  61.4 us
    unnamed x6, waiting for transfers between devices  44 us
    all_gather x2, blocking collectives, sublayer(): lax.all_gather(hidden_t, 'ra', axis=0, tiled=True)  30.1 us
    psum x2, blocking collectives, sublayer(): total_sq = lax.psum(squares, 'ra')  25.7 us
    unnamed x20, local copies, waits for them, and re-layouts  6.04 us
  transfers between devices with their start and end apart: 4, of which 4 were waited for; matrix products, arithmetic and copies ran while one was open for 0% of the time, Pallas kernels for 0%

commit v1 on v0

--- a/solution.py
+++ b/solution.py
@@ -27,7 +27,7 @@
         (((0,), (0,)), ((), ())),
         preferred_element_type=jnp.float32,
     )
-    branch = lax.psum(partial_value, "cb")
+    branch = jnp.sum(lax.all_gather(partial_value, "cb"), axis=0)
     return (0.5 * xf + 0.5 * branch).astype(jnp.bfloat16)
 
 

time: 195 us -> 164 us (0.84)
  waiting for transfers between devices: 105 us -> 74.2 us
    psum x2 -> x0, waiting for transfers between devices: 61.4 us -> none  [sublayer(): branch = lax.psum(partial_value, 'cb')]
    all_gather x0 -> x2, waiting for transfers between devices: none -> 30.2 us  [sublayer(): branch = jnp.sum(lax.all_gather(partial_value, 'cb'), axis=0)]
    reduce_sum x0 -> x2, other arithmetic: none -> 2.65 us  [sublayer(): branch = jnp.sum(lax.all_gather(partial_value, 'cb'), axis=0)]
    unnamed x20 -> x22, local copies, waits for them, and re-layouts: 6.04 us -> 6.87 us
where the time goes in v1:
time: 164 us; the launch traced here: 163 us
  waiting for transfers between devices  74.2 us (45%)
  blocking collectives  55.8 us (34%)
  between operations  13.3 us (8%)
  local copies, waits for them, and re-layouts  10.5 us (6%)
  other arithmetic  4.9 us (3%)
  matrix products  4.68 us (3%)
    unnamed x6, waiting for transfers between devices  44 us
    all_gather x2, waiting for transfers between devices, sublayer(): branch = jnp.sum(lax.all_gather(partial_value, 'cb'), axis=0)  30.2 us
    all_gather x2, blocking collectives, sublayer(): lax.all_gather(hidden_t, 'ra', axis=0, tiled=True)  30.1 us
    psum x2, blocking collectives, sublayer(): total_sq = lax.psum(squares, 'ra')  25.7 us
    unnamed x22, local copies, waits for them, and re-layouts  6.87 us
    slice x2, local copies, waits for them, and re-layouts, sublayer(): shares[:, :rows] * scale[None, :]  3.39 us
  transfers between devices with their start and end apart: 4, of which 4 were waited for; matrix products, arithmetic and copies ran while one was open for 0% of the time, Pallas kernels for 0%

profile of v1, /device:TPU:0, one launch (start us, length us, event | category | flops | bytes accessed | tf_op | source)
XLA Modules:
  0.0 163.5 jit_solution(15558211449647257783)
XLA Ops:
  6.5 0.0 copy-start
  6.5 0.0 copy-start.1
  6.5 0.0 copy-start.2
  6.5 0.0 reduce-scatter.7.cloned.1.call-start
  6.5 0.8 convert_element_type.31
  7.4 0.5 copy-done
  7.9 1.3 convolution_bitcast_fusion.2
  9.2 0.0 copy-done.1
  9.2 0.0 copy-done.2
  9.2 0.4 convolution_bitcast_fusion.3
  9.6 0.1 pad_maximum_fusion
  9.7 1.6 copy.12
  11.3 0.0 reduce-scatter.7.cloned.1.call-update
  11.3 0.0 copy-start.3
  11.3 0.0 all-gather.5.cloned.1.call-start
  11.3 0.1 fusion.1
  11.5 13.6 %psum.14 = f32[128]{0:T(128)S(1)} all-reduce(f32[128]{0:T(128)S(1)} %fusion.1), channel_id=1, replica_groups=mesh['grp'=2,'ra'=4,'cb'=4] {'ra'}, use_global_device_ids=true, to_apply=%region_2.0 | all-reduce | flops 128 | bytes 1024 | tf_op jit(solution)/shard_map/psum | solution.py:19
  25.1 22.5 %reduce-scatter.7.cloned.1.call-done = f32[352,256]{1,0:T(8,128)} async-done(((f32[1408,256]{1,0:T(8,128)}), f32[352,256]{1,0:T(8,128)}) %reduce-scatter.7.cloned.1.call-update) | async-done | bytes 360464
  47.6 1.7 %fusion.14 = (f32[352,128]{1,0:T(8,128)S(1)}, f32[352,128]{1,0:T(8,128)}) fusion(f32[352,256]{1,0:T(8,128)} %reduce-scatter.7.cloned.1.call-done), kind=kLoop, calls=%fused_computation.25 | loop fusion | bytes 720896 | tf_op jit(solution)/shard_map/slice | solution.py:22
  49.3 0.1 copy.16
  49.4 1.1 copy.17
  50.5 0.1 multiply_convert_fusion.1
  50.6 0.0 copy-start.7
  50.6 0.1 copy.10
  50.8 15.0 %all_gather.18 = bf16[1408,128]{1,0:T(8,128)(2,1)S(1)} all-gather(bf16[352,128]{1,0:T(8,128)(2,1)S(1)} %copy.10), channel_id=1, replica_groups=mesh['grp'=2,'ra'=4,'cb'=4] {'ra'}, dimensions={0}, use_global_device_ids=true | all-gather | bytes 450560 | tf_op jit(solution)/shard_map/all_gather | solution.py:25
  65.8 0.0 copy-done.3
  65.8 1.1 fusion.15
  66.9 0.0 copy-start.4
  66.9 0.0 all-gather.5.cloned.1.call-update
  66.9 0.0 reduce-scatter.9.cloned.1.call-start
  67.0 0.0 copy-done.7
  67.0 15.1 %all-gather.5.cloned.1.call-done = f32[512,512]{1,0:T(8,128)} async-done(((f32[128,512]{1,0:T(8,128)}), f32[512,512]{1,0:T(8,128)}) %all-gather.5.cloned.1.call-update) | async-done | bytes 1048592 | tf_op jit(solution)/shard_map/all_gather | solution.py:30
  82.1 1.3 reduce_sum.37
  83.4 0.0 copy-start.5
  83.4 0.1 fusion.5
  83.6 0.0 copy-done.4
  83.6 0.4 convolution_bitcast_fusion
  84.0 0.8 copy-done.5
  84.8 0.4 convolution_bitcast_fusion.1
  85.2 0.1 pad_maximum_fusion.1
  85.3 1.6 copy.14
  86.8 0.0 reduce-scatter.9.cloned.1.call-update
  86.9 0.0 copy-start.6
  86.9 0.0 all-gather.7.cloned.1.call-start
  86.9 12.1 %psum.15 = f32[128]{0:T(128)S(1)} all-reduce(f32[128]{0:T(128)S(1)} %get-tuple-element.5), channel_id=1, replica_groups=mesh['grp'=2,'ra'=4,'cb'=4] {'ra'}, use_global_device_ids=true, to_apply=%region_6.7 | all-reduce | flops 128 | bytes 1024 | tf_op jit(solution)/shard_map/psum | solution.py:19
  99.0 21.4 %reduce-scatter.9.cloned.1.call-done = f32[352,256]{1,0:T(8,128)} async-done(((f32[1408,256]{1,0:T(8,128)}), f32[352,256]{1,0:T(8,128)}) %reduce-scatter.9.cloned.1.call-update) | async-done | bytes 360464
  120.5 1.7 %fusion.13 = (f32[352,128]{1,0:T(8,128)S(1)}, f32[352,128]{1,0:T(8,128)}) fusion(f32[352,256]{1,0:T(8,128)} %reduce-scatter.9.cloned.1.call-done), kind=kLoop, calls=%fused_computation.24 | loop fusion | bytes 720896 | tf_op jit(solution)/shard_map/slice | solution.py:22
  122.2 0.1 copy.18
  122.3 1.1 copy.19
  123.3 0.1 multiply_convert_fusion
  123.5 0.1 copy.11
  123.6 15.1 %all_gather.21 = bf16[1408,128]{1,0:T(8,128)(2,1)S(1)} all-gather(bf16[352,128]{1,0:T(8,128)(2,1)S(1)} %copy.11), channel_id=1, replica_groups=mesh['grp'=2,'ra'=4,'cb'=4] {'ra'}, dimensions={0}, use_global_device_ids=true | all-gather | bytes 450560 | tf_op jit(solution)/shard_map/all_gather | solution.py:25
  138.7 0.0 copy-done.6
  138.7 1.1 fusion.16
  139.8 0.0 all-gather.7.cloned.1.call-update
  139.9 15.1 %all-gather.7.cloned.1.call-done = f32[512,512]{1,0:T(8,128)} async-done(((f32[128,512]{1,0:T(8,128)}), f32[512,512]{1,0:T(8,128)}) %all-gather.7.cloned.1.call-update) | async-done | bytes 1048592 | tf_op jit(solution)/shard_map/all_gather | solution.py:30
  154.9 1.3 reduce_sum.39
  156.3 0.7 fusion.7
  (3 shorter events, 0.0 us)
Async XLA Ops:
  6.5 1.4 copy-start
  6.5 2.7 %copy-start.1 = (bf16[128,512]{1,0:T(8,128)(2,1)S(1)}, bf16[128,512]{1,0:T(8,128)(2,1)}, u32[]{:S(2)}) copy-start(bf16[128,512]{1,0:T(8,128)(2,1)} %param.9) | copy-start | bytes 393220
  6.5 2.7 %copy-start.2 = (bf16[512,1408]{1,0:T(8,128)(2,1)S(1)}, bf16[512,1408]{1,0:T(8,128)(2,1)}, u32[]{:S(2)}) copy-start(bf16[512,1408]{1,0:T(8,128)(2,1)} %param.11) | copy-start | bytes 4325380
  6.5 41.1 %reduce-scatter.7.cloned.1.call-start = ((), (), s32[]{:S(2)}) async-start(), calls=%async_computation.4 | async-start | bytes 1802240
  11.3 54.5 %copy-start.3 = (bf16[1408,512]{1,0:T(8,128)(2,1)S(1)}, bf16[1408,512]{1,0:T(8,128)(2,1)}, u32[]{:S(2)}) copy-start(bf16[1408,512]{1,0:T(8,128)(2,1)} %param.13) | copy-start | bytes 4325380
  11.3 70.8 %all-gather.5.cloned.1.call-start = ((), (), s32[]{:S(2)}) async-start(), calls=%async_computation.2 | async-start | bytes 1310720 | tf_op jit(solution)/shard_map/all_gather | solution.py:30
  50.6 16.4 %copy-start.7 = (bf16[512]{0:T(512)(128)(2,1)S(1)}, bf16[512]{0:T(512)(128)(2,1)}, u32[]{:S(2)}) copy-start(bf16[512]{0:T(512)(128)(2,1)} %param.14) | copy-start | bytes 3076
  66.9 16.7 %copy-start.4 = (bf16[512,1408]{1,0:T(8,128)(2,1)S(1)}, bf16[512,1408]{1,0:T(8,128)(2,1)}, u32[]{:S(2)}) copy-start(bf16[512,1408]{1,0:T(8,128)(2,1)} %param.16) | copy-start | bytes 4325380
  66.9 53.5 %reduce-scatter.9.cloned.1.call-start = ((), (), s32[]{:S(2)}) async-start(), calls=%async_computation.5 | async-start | bytes 1802240
  83.4 1.4 copy-start.5
  86.9 51.8 %copy-start.6 = (bf16[1408,512]{1,0:T(8,128)(2,1)S(1)}, bf16[1408,512]{1,0:T(8,128)(2,1)}, u32[]{:S(2)}) copy-start(bf16[1408,512]{1,0:T(8,128)(2,1)} %param.17) | copy-start | bytes 4325380
  86.9 68.1 %all-gather.7.cloned.1.call-start = ((), (), s32[]{:S(2)}) async-start(), calls=%async_computation.3 | async-start | bytes 1310720 | tf_op jit(solution)/shard_map/all_gather | solution.py:30
Sparse Core Ops, SparseCore 0:
  11.4 36.1 reduce-scatter.6
  67.1 14.9 all-gather.4
  87.0 33.4 reduce-scatter.8
  140.0 14.9 all-gather.6
